TPU v7x, 32 devices: a whole 2x2x4 slice. The times are simulated.
32 devices in a mesh: sp: 8 (over z, y), tp: 4 (over x, core).
Axes of the slice: x: 2, y: 2, z: 4, core: 2. Of those that a mesh axis runs over, the one named last changes fastest.
Arguments:
- stream: bfloat16 [2048, 2048], P(('sp', 'tp')), may hold values from -6 to 6
- queries: bfloat16 [2048, 2048], P('sp', 'tp'), may hold values from -147.07821 to 147.07821
- keys: bfloat16 [2048, 2048], P('sp', 'tp'), may hold values from -7 to 7
- values: bfloat16 [2048, 2048], P('sp', 'tp'), may hold values from -6 to 6
- head_lambda: float32 [8], P('tp'), may hold values from 0.3 to 0.8
- head_gain: float32 [256], replicated, may hold values from 0.1 to 1.9
- w_out: bfloat16 [2048, 2048], P('tp'), may hold values from -0.125 to 0.125
- norm_gain: float32 [2048], replicated, may hold values from 0.1 to 1.9
- w_gate: bfloat16 [2048, 5632], P('sp', 'tp'), may hold values from -0.125 to 0.125
- w_up: bfloat16 [2048, 5632], P('sp', 'tp'), may hold values from -0.125 to 0.125
- w_down: bfloat16 [5632, 2048], P('tp', 'sp'), may hold values from -0.078125 to 0.078125
Outputs:
- result: bfloat16 [2048, 2048], P(('sp', 'tp'))
All inputs are finite; a program needn't handle non-finite values.
Results may differ from a plain program's by a relative error of at most 0.013.
Values may be sent and summed in bfloat16 or wider, within the bound.
A program may use at most 192 MiB of HBM per device.

v0:
```python
import jax
import jax.numpy as jnp
from jax import lax
from jax.sharding import PartitionSpec as P

epsilon = 1e-06


def normalize(values_in, gain):
    square_mean = jnp.mean(values_in * values_in, axis=-1, keepdims=True)
    return values_in * lax.rsqrt(square_mean + epsilon) * gain


def shards(
    stream, queries, keys, values, head_lambda, head_gain, w_out, norm_gain, w_gate, w_up, w_down
):
    row_count = queries.shape[0]
    head_count = head_lambda.shape[0]
    head_dim = queries.shape[1] // (2 * head_count)
    value_dim = values.shape[1] // head_count
    score_scale = head_dim ** (-0.5)
    offset = lax.axis_index("sp") * row_count
    query_heads = queries.reshape(row_count, head_count, 2, head_dim)
    query_pos = offset + jnp.arange(row_count, dtype=jnp.int32)
    start_state = (
        jnp.full((head_count, 2, row_count), -1e30, jnp.float32),
        jnp.zeros((head_count, 2, row_count), jnp.float32),
        jnp.zeros((head_count, 2, row_count, value_dim), jnp.float32),
    )
    key_piece = lax.all_gather(keys, "sp", axis=0, tiled=True)
    value_piece = lax.all_gather(values, "sp", axis=0, tiled=True)
    span = key_piece.shape[0]

    def update(state):
        row_max, weight_sum, partial_value = state
        key_heads = key_piece.reshape(span, head_count, 2, head_dim)
        value_heads = value_piece.reshape(span, head_count, value_dim)
        scores = (
            jnp.einsum(
                "qhsd,khsd->hsqk", query_heads, key_heads, preferred_element_type=jnp.float32
            )
            * score_scale
        )
        key_pos = jnp.arange(span, dtype=jnp.int32)
        visible = key_pos[None, :] <= query_pos[:, None]
        new_max = jnp.maximum(row_max, jnp.max(jnp.where(visible, scores, -1e30), axis=-1))
        weights = jnp.where(visible, jnp.exp(scores - new_max[..., None]), 0.0)
        new_sum = jnp.sum(weights, axis=-1)
        added = jnp.einsum(
            "hsqk,khd->hsqd",
            weights.astype(jnp.bfloat16),
            value_heads,
            preferred_element_type=jnp.float32,
        )
        return (new_max, new_sum, added)

    def unchanged(state):
        return state

    row_max, weight_sum, partial_value = lax.cond(
        jnp.int32(0) <= offset + row_count - 1, update, unchanged, start_state
    )
    map_out = partial_value / weight_sum[..., None]
    contrast = map_out[:, 0] - head_lambda[:, None, None] * map_out[:, 1]
    head_out = (
        normalize(contrast, head_gain)
        .transpose(1, 0, 2)
        .reshape(row_count, head_count * value_dim)
        .astype(jnp.bfloat16)
    )
    local_rows = stream.shape[0]
    projected = lax.psum(
        jnp.dot(head_out, w_out, preferred_element_type=jnp.float32).astype(jnp.bfloat16), "tp"
    ).astype(jnp.float32)
    stream_all = lax.all_gather(stream, "tp", axis=0, tiled=True)
    middle_all = stream_all.astype(jnp.float32) + projected
    mixer_in = normalize(middle_all, norm_gain).astype(jnp.bfloat16)
    middle = lax.dynamic_slice_in_dim(middle_all, lax.axis_index("tp") * local_rows, local_rows, 0)
    gate = jnp.dot(
        mixer_in,
        lax.all_gather(w_gate, "sp", axis=0, tiled=True),
        preferred_element_type=jnp.float32,
    )
    up_part = jnp.dot(
        mixer_in, lax.all_gather(w_up, "sp", axis=0, tiled=True), preferred_element_type=jnp.float32
    )
    down_full = lax.all_gather(w_down, "sp", axis=1, tiled=True)
    hidden = (jax.nn.silu(gate) * up_part).astype(jnp.bfloat16)
    mixed = lax.psum_scatter(
        jnp.dot(hidden, down_full, preferred_element_type=jnp.float32).astype(jnp.bfloat16),
        "tp",
        scatter_dimension=0,
        tiled=True,
    ).astype(jnp.float32)
    return (middle + mixed).astype(jnp.bfloat16)


def solution(mesh):
    placed = (
        P(("sp", "tp"), None),
        P("sp", "tp"),
        P("sp", "tp"),
        P("sp", "tp"),
        P("tp"),
        P(),
        P("tp", None),
        P(),
        P("sp", "tp"),
        P("sp", "tp"),
        P("tp", "sp"),
    )
    return jax.shard_map(
        shards, mesh=mesh, in_specs=placed, out_specs=P(("sp", "tp"), None), check_vma=False
    )
```

profile of v0, /device:TPU:0, one launch (start us, length us, event | category | flops | bytes accessed | tf_op | source)
XLA Modules:
  0.0 499.6 jit_solution(3734772541105203988)
XLA Ops:
  6.5 0.0 all-gather.11.cloned.1.call-start
  6.5 0.7 all-gather.11.cloned.1.call-update
  7.3 0.0 all-gather.9.cloned.1.call-start
  7.3 0.7 all-gather.9.cloned.1.call-update
  8.0 0.0 all-gather.7.cloned.1.call-start
  8.1 0.7 all-gather.7.cloned.1.call-update
  8.7 0.0 all-reduce.2.cloned.1.call-start
  8.8 52.5 %all-gather.11.cloned.1.call-done = bf16[2048,512]{1,0:T(8,128)(2,1)} async-done(((bf16[256,512]{1,0:T(8,128)(2,1)}), bf16[2048,512]{1,0:T(8,128)(2,1)}) %all-gather.11.cloned.1.call-update) | async-done | bytes 2097168 | tf_op jit(solution)/shard_map/all_gather | solution.py:31
  61.3 49.8 %all-gather.9.cloned.1.call-done = bf16[2048,512]{1,0:T(8,128)(2,1)} async-done(((bf16[256,512]{1,0:T(8,128)(2,1)}), bf16[2048,512]{1,0:T(8,128)(2,1)}) %all-gather.9.cloned.1.call-update) | async-done | bytes 2097168 | tf_op jit(solution)/shard_map/all_gather | solution.py:30
  111.1 28.6 %conditional.1 = (f32[2,2,256]{2,1,0:T(2,128)S(1)}, f32[2,2,256,256]{2,3,0,1:T(8,128)S(1)}) conditional(s32[]{:T(128)} %convert_element_type.40, () %tuple.13, (s32[]{:T(128)}, s32[256]{0:T(256)S(1)}, bf16[256,512]{1,0:T(8,128)(2,1)}, bf16[2048,512]{1,0:T(8,128)(2,1)}, bf16[2048,512]{1,0:T(8,128)(2,1)}) %tuple.14), branch_computations={%region_0.0_spmd, %region_1.4_spmd} | conditional | flops 1634204928 | bytes 46951500 | solution.py:60
  111.1 0.4 iota_compare_fusion
  111.5 0.0 copy-start.3
  111.5 4.2 reshape.34
  115.7 0.0 copy-done.3
  115.7 0.1 reshape.33
  115.8 6.8 %select_reduce_fusion = (f32[2,2,256]{2,1,0:T(2,128)S(1)}, f32[2,2,256,2048]{3,2,1,0:T(8,128)}) fusion(pred[256,2048]{1,0:T(8,128)(4,1)S(1)} %iota_compare_fusion, bf16[2048,2,2,128]{3,2,1,0:T(2,128)(2,1)} %reshape.34, bf16[256,2,2,128]{3,2,1,0:T(2,128)(2,1)S(1)} %reshape.33), kind=kOutput, calls=%fused_computation.1 | convolution fusion | flops 543161344 | bytes 11276288 | tf_op jit(solution)/shard_map/cond/branch_1_fun/qhsd,khsd->hsqk/dot_general | solution.py:39
  122.6 4.0 reshape.35
  126.6 6.8 %fusion.2 = f32[2,2,256,256]{3,2,1,0:T(8,128)} fusion(f32[2,2,256,2048]{3,2,1,0:T(8,128)} %get-tuple-element.31, f32[2,2,256]{2,1,0:T(2,128)S(1)} %broadcast_maximum_fusion, pred[256,2048]{1,0:T(8,128)(4,1)S(1)} %iota_compare_fusion, bf16[2048,2,256,1]{2,1,0,3:T(2,128)(2,1)} %bitcast.27), kind=kOutput, calls=%fused_computation.4 | convolution fusion | flops 1082130432 | bytes 12062720 | tf_op jit(solution)/shard_map/cond/branch_1_fun/hsqk,khd->hsqd/dot_general | solution.py:49
  133.4 1.6 copy.26
  134.9 4.7 fusion.1
  139.6 0.0 copy-start.4
  139.7 0.0 copy-start.5
  139.7 0.1 broadcast_divide_fusion
  139.8 0.5 copy-done.4
  140.3 0.2 multiply_reduce_fusion.1
  140.5 0.0 copy-done.5
  140.5 0.2 multiply_convert_fusion.1
  140.6 1.7 convolution_convert_fusion
  142.4 0.0 all-reduce.2.cloned.1.call-update
  142.4 0.0 all-gather.13.cloned.1.call-start
  142.4 0.5 all-gather.13.cloned.1.call-update
  143.0 0.0 all-gather.15.cloned.1.call-start
  143.0 0.5 all-gather.15.cloned.1.call-update
  143.6 0.0 all-gather.17.cloned.1.call-start
  143.6 0.7 all-gather.17.cloned.1.call-update
  144.3 0.0 copy-start.6
  144.3 0.2 reduce-scatter.2.cloned.1.call-start
  144.6 0.0 all-gather.7.cloned.1.call-done
  144.6 32.8 %all-reduce.2.cloned.1.call-done = bf16[256,2048]{1,0:T(8,128)(2,1)} async-done(((bf16[256,2048]{1,0:T(8,128)(2,1)}), bf16[256,2048]{1,0:T(8,128)(2,1)}) %all-reduce.2.cloned.1.call-update) | async-done | bytes 1048592 | tf_op jit(solution)/shard_map/psum | solution.py:72
  177.3 3.2 convert_add_fusion
  180.6 91.6 %all-gather.13.cloned.1.call-done = bf16[2048,1408]{1,0:T(8,128)(2,1)} async-done(((bf16[256,1408]{1,0:T(8,128)(2,1)}), bf16[2048,1408]{1,0:T(8,128)(2,1)}) %all-gather.13.cloned.1.call-update) | async-done | bytes 5767184 | tf_op jit(solution)/shard_map/all_gather | solution.py:81
  272.2 5.9 %fusion.18 = f32[256,1408]{1,0:T(8,128)} fusion(bf16[2048,1408]{1,0:T(8,128)(2,1)} %all-gather.13.cloned.1.call-done, f32[2048]{0:T(1024)S(1)} %copy-done.6, f32[256]{0:T(256)S(1)} %add_rsqrt_fusion.1, bf16[256,2048]{1,0:T(8,128)(2,1)} %all-reduce.2.cloned.1.call-done, bf16[256,2048]{1,0:T(8,128)(2,1)S(1)} %copy-done.2), kind=kOutput, calls=%fused_computation.36 | convolution fusion | flops 1479540736 | bytes 9315328 | tf_op jit(solution)/shard_map/dot_general | solution.py:79
  278.1 86.6 %all-gather.15.cloned.1.call-done = bf16[2048,1408]{1,0:T(8,128)(2,1)} async-done(((bf16[256,1408]{1,0:T(8,128)(2,1)}), bf16[2048,1408]{1,0:T(8,128)(2,1)}) %all-gather.15.cloned.1.call-update) | async-done | bytes 5767184 | tf_op jit(solution)/shard_map/all_gather | solution.py:85
  364.8 93.4 %all-gather.17.cloned.1.call-done = bf16[1408,2048]{1,0:T(8,128)(2,1)} async-done(((bf16[1408,256]{1,0:T(8,128)(2,1)}), bf16[1408,2048]{1,0:T(8,128)(2,1)}) %all-gather.17.cloned.1.call-update) | async-done | bytes 5767184 | tf_op jit(solution)/shard_map/all_gather | solution.py:87
  458.1 9.6 %convolution_convert_fusion.1 = bf16[256,2048]{1,0:T(8,128)(2,1)} fusion(bf16[1408,2048]{1,0:T(8,128)(2,1)} %all-gather.17.cloned.1.call-done, bf16[2048,1408]{1,0:T(8,128)(2,1)} %all-gather.15.cloned.1.call-done, f32[256,1408]{1,0:T(8,128)} %fusion.18, f32[2048]{0:T(1024)S(1)} %copy-done.6, f32[256]{0:T(256)S(1)} %add_rsqrt_fusion.1, ...), kind=kOutput, calls=%fused_computation.21 | convolution fusion | flops 2958622720 | bytes 16131072 | tf_op jit(solution)/shard_map/dot_general | solution.py:90
  467.8 0.0 reduce-scatter.2.cloned.1.call-update
  467.8 23.1 %reduce-scatter.2.cloned.1.call-done = bf16[64,2048]{1,0:T(8,128)(2,1)} async-done(((bf16[256,2048]{1,0:T(8,128)(2,1)}), bf16[64,2048]{1,0:T(8,128)(2,1)}) %reduce-scatter.2.cloned.1.call-update) | async-done | bytes 262160 | tf_op jit(solution)/shard_map/reduce_scatter | solution.py:89
  490.9 1.9 add_convert_fusion
  (13 shorter events, 0.1 us)
Async XLA Ops:
  6.5 134.1 %copy-start = (bf16[512,2048]{1,0:T(8,128)(2,1)S(1)}, bf16[512,2048]{1,0:T(8,128)(2,1)}, u32[]{:S(2)}) copy-start(bf16[512,2048]{1,0:T(8,128)(2,1)} %param.19) | copy-start | bytes 6291460
  6.5 54.8 %all-gather.11.cloned.1.call-start = ((), (), s32[]{:S(2)}) async-start(), calls=%async_computation.3 | async-start | bytes 2359296 | tf_op jit(solution)/shard_map/all_gather | solution.py:31
  7.3 103.8 %all-gather.9.cloned.1.call-start = ((), (), s32[]{:S(2)}) async-start(), calls=%async_computation.2 | async-start | bytes 2359296 | tf_op jit(solution)/shard_map/all_gather | solution.py:30
  8.0 136.6 %all-gather.7.cloned.1.call-start = ((), (), s32[]{:S(2)}) async-start(), calls=%async_computation.1 | async-start | bytes 1310720 | tf_op jit(solution)/shard_map/all_gather | solution.py:75
  8.7 168.6 %all-reduce.2.cloned.1.call-start = ((), (), s32[]{:S(2)}) async-start(), calls=%async_computation.4 | async-start | bytes 2097152 | tf_op jit(solution)/shard_map/psum | solution.py:72
  111.5 15.2 %copy-start.1 = (pred[256,2048]{1,0:T(8,128)(4,1)}, pred[256,2048]{1,0:T(8,128)(4,1)S(1)}, u32[]{:S(2)}) copy-start(pred[256,2048]{1,0:T(8,128)(4,1)S(1)} %iota_compare_fusion) | copy-start | bytes 1572868 | tf_op jit(solution)/shard_map/cond
  111.5 4.2 copy-start.3
  139.6 0.7 copy-start.4
  139.7 0.8 copy-start.5
  142.4 129.8 %all-gather.13.cloned.1.call-start = ((), (), s32[]{:S(2)}) async-start(), calls=%async_computation.5 | async-start | bytes 6488064 | tf_op jit(solution)/shard_map/all_gather | solution.py:81
  143.0 221.8 %all-gather.15.cloned.1.call-start = ((), (), s32[]{:S(2)}) async-start(), calls=%async_computation.6 | async-start | bytes 6488064 | tf_op jit(solution)/shard_map/all_gather | solution.py:85
  143.6 314.6 %all-gather.17.cloned.1.call-start = ((), (), s32[]{:S(2)}) async-start(), calls=%async_computation.7 | async-start | bytes 6488064 | tf_op jit(solution)/shard_map/all_gather | solution.py:87
  144.3 127.9 %copy-start.6 = (f32[2048]{0:T(1024)S(1)}, f32[2048]{0:T(1024)}, u32[]{:S(2)}) copy-start(f32[2048]{0:T(1024)} %param.20) | copy-start | bytes 24580
  144.3 346.6 %reduce-scatter.2.cloned.1.call-start = ((), (), s32[]{:S(2)}) async-start(), calls=%async_computation.8 | async-start | bytes 1310720 | tf_op jit(solution)/shard_map/reduce_scatter | solution.py:89
  144.6 127.6 %copy-start.2 = (bf16[256,2048]{1,0:T(8,128)(2,1)S(1)}, bf16[256,2048]{1,0:T(8,128)(2,1)}, u32[]{:S(2)}) copy-start(bf16[256,2048]{1,0:T(8,128)(2,1)} %all-gather.7.cloned.1.call-done) | copy-start | bytes 3145732
Sparse Core Ops, SparseCore 0:
  9.5 51.7 all-gather.10
  63.4 47.6 all-gather.8
  112.6 15.2 all-gather.6
  142.5 34.7 all-reduce.1
  179.4 92.7 all-gather.12
  274.2 90.4 all-gather.14
  366.8 91.2 all-gather.16
  467.9 22.9 reduce-scatter.1
where the time goes:
time: 500 us
  waiting for transfers between devices  434 us (87%)
  matrix products  30.9 us (6%)
  between operations  13.6 us (3%)
  other arithmetic  10.6 us (2%)
  local copies, waits for them, and re-layouts  10.4 us (2%)
    all_gather x1, waiting for transfers between devices, shards(): down_full = lax.all_gather(w_down, 'sp', axis=1, tiled=True)  93.4 us
    all_gather x1, waiting for transfers between devices, shards(): lax.all_gather(w_gate, 'sp', axis=0, tiled=True)  91.6 us
    all_gather x1, waiting for transfers between devices, shards(): lax.all_gather(w_up, 'sp', axis=0, tiled=True)  86.6 us
    all_gather x1, waiting for transfers between devices, shards(): value_piece = lax.all_gather(values, 'sp', axis=0, tiled=True)  52.5 us
    all_gather x1, waiting for transfers between devices, shards(): key_piece = lax.all_gather(keys, 'sp', axis=0, tiled=True)  49.8 us
    psum x1, waiting for transfers between devices, shards(): lax.psum(jnp.dot(head_out, w_out, preferred_element_type=jnp.float32).ast...  32.8 us
    reduce_scatter x1, waiting for transfers between devices, shards(): lax.psum_scatter(jnp.dot(hidden, down_full, preferred_element_type=jnp.fl...  23.1 us
  transfers between devices with their start and end apart: 8, of which 7 were waited for; matrix products, arithmetic and copies ran while one was open for 8% of the time, Pallas kernels for 0%

commit v1 on v0

--- a/solution.py
+++ b/solution.py
@@ -4,6 +4,12 @@
 from jax.sharding import PartitionSpec as P
 
 epsilon = 1e-06
+
+
+def gather_and_add(shard, axis):
+    terms = lax.all_gather(shard, axis, axis=0, tiled=False)
+    summed = terms.sum(axis=0)
+    return summed
 
 
 def normalize(values_in, gain):
@@ -69,7 +75,7 @@
         .astype(jnp.bfloat16)
     )
     local_rows = stream.shape[0]
-    projected = lax.psum(
+    projected = gather_and_add(
         jnp.dot(head_out, w_out, preferred_element_type=jnp.float32).astype(jnp.bfloat16), "tp"
     ).astype(jnp.float32)
     stream_all = lax.all_gather(stream, "tp", axis=0, tiled=True)

time: 500 us -> 516 us (1.032)
  waiting for transfers between devices: 434 us -> 447 us
    psum x1 -> x0, waiting for transfers between devices: 32.8 us -> none  [shards(): lax.psum(jnp.dot(head_out, w_out, preferred_element_type=jnp.float32).ast...]
    all_gather x0 -> x1, waiting for transfers between devices: none -> 30.4 us  [gather_and_add(): terms = lax.all_gather(shard, axis, axis=0, tiled=False)]
    all_gather x1, waiting for transfers between devices: 0.02 us -> 15.1 us  [shards(): stream_all = lax.all_gather(stream, 'tp', axis=0, tiled=True)]
  transfers between devices with their start and end apart: 8 -> 8, of which waited for: 7 -> 8; matrix products, arithmetic and copies ran while one was open for 8% -> 2% of each run, Pallas kernels for 0% -> 0%
where the time goes in v1:
time: 516 us; the launch traced here: 515 us
  waiting for transfers between devices  447 us (87%)
  matrix products  30.8 us (6%)
  between operations  13.6 us (3%)
  other arithmetic  13.3 us (3%)
  local copies, waits for them, and re-layouts  10.4 us (2%)
    all_gather x1, waiting for transfers between devices, shards(): down_full = lax.all_gather(w_down, 'sp', axis=1, tiled=True)  93.4 us
    all_gather x1, waiting for transfers between devices, shards(): lax.all_gather(w_gate, 'sp', axis=0, tiled=True)  91.5 us
    all_gather x1, waiting for transfers between devices, shards(): lax.all_gather(w_up, 'sp', axis=0, tiled=True)  86.6 us
    all_gather x1, waiting for transfers between devices, shards(): key_piece = lax.all_gather(keys, 'sp', axis=0, tiled=True)  53.2 us
    all_gather x1, waiting for transfers between devices, shards(): value_piece = lax.all_gather(values, 'sp', axis=0, tiled=True)  49.8 us
    all_gather x1, waiting for transfers between devices, gather_and_add(): terms = lax.all_gather(shard, axis, axis=0, tiled=False)  30.4 us
    reduce_scatter x1, waiting for transfers between devices, shards(): lax.psum_scatter(jnp.dot(hidden, down_full, preferred_element_type=jnp.fl...  23.1 us
    all_gather x1, waiting for transfers between devices, shards(): stream_all = lax.all_gather(stream, 'tp', axis=0, tiled=True)  15.1 us
  transfers between devices with their start and end apart: 8, of which 8 were waited for; matrix products, arithmetic and copies ran while one was open for 2% of the time, Pallas kernels for 0%

profile of v1, /device:TPU:0, one launch (start us, length us, event | category | flops | bytes accessed | tf_op | source)
XLA Modules:
  0.0 515.4 jit_solution(10457912026612638012)
XLA Ops:
  6.5 0.0 copy-start
  6.5 0.0 all-gather.11.cloned.1.call-start
  6.5 0.7 all-gather.11.cloned.1.call-update
  7.3 0.0 all-gather.13.cloned.1.call-start
  7.3 0.7 all-gather.13.cloned.1.call-update
  8.0 0.0 all-gather.21.cloned.1.call-start
  8.1 53.2 %all-gather.11.cloned.1.call-done = bf16[2048,512]{1,0:T(8,128)(2,1)} async-done(((bf16[256,512]{1,0:T(8,128)(2,1)}), bf16[2048,512]{1,0:T(8,128)(2,1)}) %all-gather.11.cloned.1.call-update) | async-done | bytes 2097168 | tf_op jit(solution)/shard_map/all_gather | solution.py:36
  61.3 49.8 %all-gather.13.cloned.1.call-done = bf16[2048,512]{1,0:T(8,128)(2,1)} async-done(((bf16[256,512]{1,0:T(8,128)(2,1)}), bf16[2048,512]{1,0:T(8,128)(2,1)}) %all-gather.13.cloned.1.call-update) | async-done | bytes 2097168 | tf_op jit(solution)/shard_map/all_gather | solution.py:37
  111.1 28.5 %conditional.1 = (f32[2,2,256]{2,1,0:T(2,128)S(1)}, f32[2,2,256,256]{2,3,0,1:T(8,128)S(1)}) conditional(s32[]{:T(128)} %convert_element_type.42, () %tuple.13, (s32[]{:T(128)}, s32[256]{0:T(256)S(1)}, bf16[256,512]{1,0:T(8,128)(2,1)}, bf16[2048,512]{1,0:T(8,128)(2,1)}, bf16[2048,512]{1,0:T(8,128)(2,1)}) %tuple.14), branch_computations={%region_0.0_spmd, %region_1.4_spmd} | conditional | flops 1634204928 | bytes 46951500 | solution.py:66
  111.1 0.4 iota_compare_fusion
  111.5 0.0 copy-start.2
  111.5 4.2 reshape.34
  115.7 0.1 reshape.33
  115.7 6.8 %select_reduce_fusion = (f32[2,2,256]{2,1,0:T(2,128)S(1)}, f32[2,2,256,2048]{3,2,1,0:T(8,128)}) fusion(pred[256,2048]{1,0:T(8,128)(4,1)S(1)} %iota_compare_fusion, bf16[2048,2,2,128]{3,2,1,0:T(2,128)(2,1)} %reshape.34, bf16[256,2,2,128]{3,2,1,0:T(2,128)(2,1)S(1)} %reshape.33), kind=kOutput, calls=%fused_computation.1 | convolution fusion | flops 543161344 | bytes 11276288 | tf_op jit(solution)/shard_map/cond/branch_1_fun/qhsd,khsd->hsqk/dot_general | solution.py:45
  122.6 4.0 reshape.35
  126.6 6.7 %fusion.2 = f32[2,2,256,256]{3,2,1,0:T(8,128)} fusion(f32[2,2,256,2048]{3,2,1,0:T(8,128)} %get-tuple-element.31, f32[2,2,256]{2,1,0:T(2,128)S(1)} %broadcast_maximum_fusion, pred[256,2048]{1,0:T(8,128)(4,1)S(1)} %iota_compare_fusion, bf16[2048,2,256,1]{2,1,0,3:T(2,128)(2,1)} %bitcast.29), kind=kOutput, calls=%fused_computation.4 | convolution fusion | flops 1082130432 | bytes 12062720 | tf_op jit(solution)/shard_map/cond/branch_1_fun/hsqk,khd->hsqd/dot_general | solution.py:55
  133.3 1.6 copy.26
  134.9 4.7 fusion.1
  139.6 0.0 copy-start.3
  139.6 0.0 copy-start.4
  139.6 0.1 broadcast_divide_fusion
  139.7 0.5 copy-done.3
  140.2 0.2 multiply_reduce_fusion.1
  140.4 0.1 multiply_convert_fusion.1
  140.6 1.7 convolution_convert_fusion
  142.3 0.0 all-gather.21.cloned.1.call-update
  142.3 0.0 all-gather.9.cloned.1.call-start
  142.3 0.5 all-gather.9.cloned.1.call-update
  142.9 0.0 all-gather.15.cloned.1.call-start
  142.9 0.5 all-gather.15.cloned.1.call-update
  143.4 0.0 all-gather.17.cloned.1.call-start
  143.5 0.5 all-gather.17.cloned.1.call-update
  144.0 0.0 all-gather.19.cloned.1.call-start
  144.1 0.7 all-gather.19.cloned.1.call-update
  144.8 0.2 reduce-scatter.2.cloned.1.call-start
  145.0 30.4 %all-gather.21.cloned.1.call-done = bf16[1024,2048]{1,0:T(8,128)(2,1)} async-done(((bf16[256,2048]{1,0:T(8,128)(2,1)}), bf16[1024,2048]{1,0:T(8,128)(2,1)}) %all-gather.21.cloned.1.call-update) | async-done | bytes 4194320 | tf_op jit(solution)/shard_map/all_gather | solution.py:10
  175.4 3.1 reduce_sum.40
  178.5 0.0 copy-start.5
  178.5 15.1 %all-gather.9.cloned.1.call-done = bf16[256,2048]{1,0:T(8,128)(2,1)} async-done(((bf16[64,2048]{1,0:T(8,128)(2,1)}), bf16[256,2048]{1,0:T(8,128)(2,1)}) %all-gather.9.cloned.1.call-update) | async-done | bytes 1048592 | tf_op jit(solution)/shard_map/all_gather | solution.py:81
  193.6 2.9 convert_add_fusion
  196.5 91.5 %all-gather.15.cloned.1.call-done = bf16[2048,1408]{1,0:T(8,128)(2,1)} async-done(((bf16[256,1408]{1,0:T(8,128)(2,1)}), bf16[2048,1408]{1,0:T(8,128)(2,1)}) %all-gather.15.cloned.1.call-update) | async-done | bytes 5767184 | tf_op jit(solution)/shard_map/all_gather | solution.py:87
  288.0 5.9 %fusion.18 = f32[256,1408]{1,0:T(8,128)} fusion(bf16[2048,1408]{1,0:T(8,128)(2,1)} %all-gather.15.cloned.1.call-done, f32[2048]{0:T(1024)S(1)} %copy-done.5, f32[256]{0:T(256)S(1)} %add_rsqrt_fusion.1, bf16[256,2048]{1,0:T(8,128)(2,1)S(1)} %reduce_sum.40, bf16[256,2048]{1,0:T(8,128)(2,1)} %all-gather.9.cloned.1.call-done), kind=kOutput, calls=%fused_computation.36 | convolution fusion | flops 1479540736 | bytes 9315328 | tf_op jit(solution)/shard_map/dot_general | solution.py:85
  293.9 86.6 %all-gather.17.cloned.1.call-done = bf16[2048,1408]{1,0:T(8,128)(2,1)} async-done(((bf16[256,1408]{1,0:T(8,128)(2,1)}), bf16[2048,1408]{1,0:T(8,128)(2,1)}) %all-gather.17.cloned.1.call-update) | async-done | bytes 5767184 | tf_op jit(solution)/shard_map/all_gather | solution.py:91
  380.5 93.4 %all-gather.19.cloned.1.call-done = bf16[1408,2048]{1,0:T(8,128)(2,1)} async-done(((bf16[1408,256]{1,0:T(8,128)(2,1)}), bf16[1408,2048]{1,0:T(8,128)(2,1)}) %all-gather.19.cloned.1.call-update) | async-done | bytes 5767184 | tf_op jit(solution)/shard_map/all_gather | solution.py:93
  473.9 9.7 %convolution_convert_fusion.1 = bf16[256,2048]{1,0:T(8,128)(2,1)} fusion(bf16[1408,2048]{1,0:T(8,128)(2,1)} %all-gather.19.cloned.1.call-done, bf16[2048,1408]{1,0:T(8,128)(2,1)} %all-gather.17.cloned.1.call-done, f32[256,1408]{1,0:T(8,128)} %fusion.18, f32[2048]{0:T(1024)S(1)} %copy-done.5, f32[256]{0:T(256)S(1)} %add_rsqrt_fusion.1, ...), kind=kOutput, calls=%fused_computation.21 | convolution fusion | flops 2958622720 | bytes 16131072 | tf_op jit(solution)/shard_map/dot_general | solution.py:96
  483.6 0.0 reduce-scatter.2.cloned.1.call-update
  483.6 23.1 %reduce-scatter.2.cloned.1.call-done = bf16[64,2048]{1,0:T(8,128)(2,1)} async-done(((bf16[256,2048]{1,0:T(8,128)(2,1)}), bf16[64,2048]{1,0:T(8,128)(2,1)}) %reduce-scatter.2.cloned.1.call-update) | async-done | bytes 262160 | tf_op jit(solution)/shard_map/reduce_scatter | solution.py:95
  506.7 1.9 add_convert_fusion
  (12 shorter events, 0.0 us)
Async XLA Ops:
  6.5 134.0 %copy-start = (bf16[512,2048]{1,0:T(8,128)(2,1)S(1)}, bf16[512,2048]{1,0:T(8,128)(2,1)}, u32[]{:S(2)}) copy-start(bf16[512,2048]{1,0:T(8,128)(2,1)} %param.19) | copy-start | bytes 6291460
  6.5 54.8 %all-gather.11.cloned.1.call-start = ((), (), s32[]{:S(2)}) async-start(), calls=%async_computation.2 | async-start | bytes 2359296 | tf_op jit(solution)/shard_map/all_gather | solution.py:36
  7.3 103.8 %all-gather.13.cloned.1.call-start = ((), (), s32[]{:S(2)}) async-start(), calls=%async_computation.3 | async-start | bytes 2359296 | tf_op jit(solution)/shard_map/all_gather | solution.py:37
  8.0 167.4 %all-gather.21.cloned.1.call-start = ((), (), s32[]{:S(2)}) async-start(), calls=%async_computation.8 | async-start | bytes 5242880 | tf_op jit(solution)/shard_map/all_gather | solution.py:10
  111.5 15.1 %copy-start.1 = (pred[256,2048]{1,0:T(8,128)(4,1)}, pred[256,2048]{1,0:T(8,128)(4,1)S(1)}, u32[]{:S(2)}) copy-start(pred[256,2048]{1,0:T(8,128)(4,1)S(1)} %iota_compare_fusion) | copy-start | bytes 1572868 | tf_op jit(solution)/shard_map/cond
  111.5 4.2 copy-start.2
  139.6 0.7 copy-start.3
  139.6 0.8 copy-start.4
  142.3 51.3 %all-gather.9.cloned.1.call-start = ((), (), s32[]{:S(2)}) async-start(), calls=%async_computation.1 | async-start | bytes 1310720 | tf_op jit(solution)/shard_map/all_gather | solution.py:81
  142.9 145.1 %all-gather.15.cloned.1.call-start = ((), (), s32[]{:S(2)}) async-start(), calls=%async_computation.4 | async-start | bytes 6488064 | tf_op jit(solution)/shard_map/all_gather | solution.py:87
  143.4 237.1 %all-gather.17.cloned.1.call-start = ((), (), s32[]{:S(2)}) async-start(), calls=%async_computation.5 | async-start | bytes 6488064 | tf_op jit(solution)/shard_map/all_gather | solution.py:91
  144.0 329.9 %all-gather.19.cloned.1.call-start = ((), (), s32[]{:S(2)}) async-start(), calls=%async_computation.6 | async-start | bytes 6488064 | tf_op jit(solution)/shard_map/all_gather | solution.py:93
  144.8 361.9 %reduce-scatter.2.cloned.1.call-start = ((), (), s32[]{:S(2)}) async-start(), calls=%async_computation.7 | async-start | bytes 1310720 | tf_op jit(solution)/shard_map/reduce_scatter | solution.py:95
  178.5 109.4 %copy-start.5 = (f32[2048]{0:T(1024)S(1)}, f32[2048]{0:T(1024)}, u32[]{:S(2)}) copy-start(f32[2048]{0:T(1024)} %param.20) | copy-start | bytes 24580
Sparse Core Ops, SparseCore 0:
  9.5 51.7 all-gather.10
  63.4 47.6 all-gather.12
  142.4 32.9 all-gather.20
  176.8 16.6 all-gather.8
  195.6 92.3 all-gather.14
  290.0 90.4 all-gather.16
  382.6 91.2 all-gather.18
  483.7 22.9 reduce-scatter.1
